TPU v7x, 32 devices: a whole 2x2x4 slice. The times are simulated.
32 devices in a mesh: fs: 16 (over z, y, x), tp: 2 (over core).
Axes of the slice: x: 2, y: 2, z: 4, core: 2. Of those that a mesh axis runs over, the one named last changes fastest.
Arguments:
- inputs: bfloat16 [8192, 2048], P('fs', 'tp'), may hold values from -6 to 6
- value_cotangent: bfloat16 [8192, 2048], P('fs', 'tp'), may hold values from -6 to 6
- first_map: bfloat16 [8192, 2048], P('fs', 'tp'), may hold values from -6 to 6
- second_map: bfloat16 [8192, 2048], P('fs', 'tp'), may hold values from -6 to 6
- lambdas: float32 [16], P('tp'), may hold values from 0.3 to 0.8
- head_gain: float32 [128], replicated, may hold values from 0.1 to 1.9
- output_cotangent: bfloat16 [8192, 2048], P('fs', 'tp'), may hold values from -6 to 6
- value_factor: bfloat16 [2048, 256], replicated, may hold values from -0.125 to 0.125
- output_factor: bfloat16 [2048, 256], replicated, may hold values from -0.125 to 0.125
- value_weight: float32 [2048, 2048], P('fs', 'tp'), may hold values from -0.125 to 0.125
- output_weight: float32 [2048, 2048], P('tp', 'fs'), may hold values from -0.125 to 0.125
- value_moment: float32 [256, 2048], P('fs', 'tp'), may hold values from -6 to 6
- value_second: float32 [256, 2048], P('fs', 'tp'), may hold values from 0.25 to 4
- output_moment: float32 [256, 2048], P('fs', 'tp'), may hold values from -6 to 6
- output_second: float32 [256, 2048], P('fs', 'tp'), may hold values from 0.25 to 4
Outputs:
- value_master: float32 [2048, 2048], P('fs', 'tp')
- output_master: float32 [2048, 2048], P('tp', 'fs')
- value_moment_new: float32 [256, 2048], P('fs', 'tp')
- value_second_new: float32 [256, 2048], P('fs', 'tp')
- output_moment_new: float32 [256, 2048], P('fs', 'tp')
- output_second_new: float32 [256, 2048], P('fs', 'tp')
- value_copy: bfloat16 [2048, 2048], P(None, 'tp')
- output_copy: bfloat16 [2048, 2048], P('tp')
All inputs are finite; a program needn't handle non-finite values.
Results may differ from a plain program's by a relative error of at most 0.0027.
Values may be sent and summed in bfloat16 or wider, within the bound.
A program may use at most 64 MiB of HBM per device.

v0:
```python
import functools
import math

import jax
import jax.numpy as jnp
from jax import lax
from jax.experimental import pallas as pl
from jax.experimental.pallas import tpu as pltpu
from jax.sharding import PartitionSpec as P

F32 = jnp.float32
BF16 = jnp.bfloat16


CODE = 2.0**30


def encode(w):
    square = (w * CODE) * (w * CODE)
    fourth = square * square
    return jnp.where(w < 0, -fourth, fourth).astype(BF16)


def decode(v):
    v = v.astype(F32)
    size = lax.rsqrt(lax.rsqrt(jnp.maximum(jnp.abs(v), 1e-36))) * (1.0 / CODE)
    return jnp.where(v < 0, -size, size)


def exchange(
    nfs, ntp, scale,
    vw_in, ow_in, inp_in, ocot_in, first_in, second_in, vcot_in, lam, gain, vfac, ofac,
    vm, vs, om, os_,
    gv, go, dfull, own_out,
    vw, ow, inp, ocot, first, second, vcot, heads, proj, part, got, direction,
    vsend, vrecv, osend, orecv, psend, precv, rsend, rrecv,
    dvsend, dvrecv, dosend, dorecv, lsem, insem,
):
    me = lax.axis_index("fs")
    tp = lax.axis_index("tp")
    cols = inp.shape[1]
    rank = vfac.shape[1]
    nx = 2 if nfs % 2 == 0 else 1
    ny = 2 if nfs % 4 == 0 else 1
    nz = nfs // (nx * ny)
    x = lax.rem(me, nx)
    y = lax.rem(lax.div(me, nx), ny)
    z = lax.div(me, nx * ny)

    def at(dz, dy, dx):
        zz = lax.rem(z + dz, nz)
        yy = lax.rem(y + dy, ny)
        xx = lax.rem(x + dx, nx)
        return (zz * ny + yy) * nx + xx

    barrier = pltpu.get_barrier_semaphore()
    for k in range(1, nfs):
        pl.semaphore_signal(barrier, inc=1, device_id={"fs": lax.rem(me + k, nfs)})
    for k in range(1, ntp):
        pl.semaphore_signal(barrier, inc=1, device_id={"tp": lax.rem(tp + k, ntp)})
    loads = []
    pairs = ((inp_in, inp), (ocot_in, ocot), (first_in, first), (second_in, second), (vcot_in, vcot))
    for k, (src, dst) in enumerate(pairs):
        load = pltpu.make_async_copy(src, dst, insem.at[k])
        load.start()
        loads.append(load)
    vw[...] = encode(vw_in[...])
    ow[...] = encode(ow_in[...])
    pl.semaphore_wait(barrier, nfs + ntp - 2)

    width = vw.shape[0]

    def vslot(b):
        return gv.at[b]

    def oslot(b):
        if len(go.shape) == 2:
            return go.at[:, pl.ds(pl.multiple_of(b * width, width), width)]
        return go.at[b]

    def dvslot(b):
        return dfull.at[b, :, pl.ds(0, cols)]

    def doslot(b):
        return dfull.at[b, :, pl.ds(cols, cols)]

    kinds = {
        "v": (vslot, vsend, vrecv),
        "o": (oslot, osend, orecv),
        "dv": (dvslot, dvsend, dvrecv),
        "do": (doslot, dosend, dorecv),
    }
    pending = []
    counts = {kind: 0 for kind in kinds}

    def when(cond, run):
        if cond is None:
            run()
        else:
            pl.when(cond)(run)

    def send(kind, src, b, target, cond=None):
        k = counts[kind]
        counts[kind] = k + 1
        slot, ss, rs = kinds[kind]

        def make():
            return pltpu.make_async_remote_copy(
                src_ref=slot(b) if src is None else src,
                dst_ref=slot(b),
                send_sem=ss.at[k],
                recv_sem=rs.at[b],
                device_id={"fs": target},
            )

        when(cond, lambda: make().start())
        pending.append((cond, make))

    def arrived(kind, b, cond=None):
        slot, ss, rs = kinds[kind]
        when(cond, lambda: pltpu.make_async_remote_copy(
            src_ref=slot(b), dst_ref=slot(b), send_sem=ss.at[0], recv_sem=rs.at[b],
            device_id={"fs": me},
        ).wait_recv())

    def spread(kind, src, b, cond=None):
        turns = ((ny, (0, 1, 0)), (nx, (0, 0, 1)))
        for extent, turn in turns if kind in ("v", "dv") else turns[::-1]:
            if extent > 1:
                send(kind, src, b, at(*turn), cond)

    def across(kind, bz, cond=None):
        first_turn, second_turn = (ny, nx) if kind in ("v", "dv") else (nx, ny)
        if first_turn == 1:
            return
        if kind in ("v", "dv"):
            b, target = (bz * ny + lax.rem(y + 1, ny)) * nx + x, at(0, 0, 1)
        else:
            b, target = (bz * ny + y) * nx + lax.rem(x + 1, nx), at(0, 1, 0)
        arrived(kind, b, cond)
        if second_turn > 1:
            send(kind, None, b, target, cond)

    def plane(bz):
        return (bz * ny + y) * nx + x

    up, down = lax.rem(z + 1, nz), lax.rem(z + nz - 1, nz)

    def along(kind, s):
        for sign in (1, -1):
            source = z - sign * s
            cond = source >= 0 if sign == 1 else source < nz
            b = plane(lax.rem(source + nz, nz))
            arrived(kind, b, cond)
            if sign == 1:
                send(kind, None, b, plane(up), (source >= 0) & (z + 1 < nz))
            else:
                send(kind, None, b, plane(down), (source < nz) & (z > 0))
            spread(kind, None, b, cond)

    def behind(kind, s):
        for sign in (1, -1):
            source = z - sign * s
            cond = source >= 0 if sign == 1 else source < nz
            across(kind, lax.rem(source + nz, nz), cond)

    own_v = pltpu.make_async_copy(vw, vslot(me), lsem.at[0])
    own_o = pltpu.make_async_copy(ow, oslot(me), lsem.at[1])
    own_v.start()
    own_o.start()
    for kind, src in (("v", vw), ("o", ow)):
        send(kind, src, me, plane(up), z + 1 < nz)
        send(kind, src, me, plane(down), z > 0)
        spread(kind, src, me)

    mine = pl.ds(pl.multiple_of(tp * cols, cols), cols)
    loads[0].wait()
    proj[0, :, :rank] = jnp.dot(inp[...], vfac[mine, :], preferred_element_type=F32)
    loads[1].wait()
    proj[0, :, rank:] = jnp.dot(ocot[...], ofac[mine, :], preferred_element_type=F32)
    pcopies = []
    for k in range(1, ntp):
        copy = pltpu.make_async_remote_copy(
            src_ref=proj.at[0], dst_ref=proj.at[k],
            send_sem=psend.at[k], recv_sem=precv.at[k],
            device_id={"tp": lax.rem(tp + k, ntp)},
        )
        copy.start()
        pcopies.append(copy)

    loads[2].wait()
    loads[3].wait()
    head_width = gain.shape[1]
    for h in range(cols // head_width):
        span = pl.ds(h * head_width, head_width)
        diff = first[:, span].astype(F32) - lam[h] * second[:, span].astype(F32)
        mean = jnp.mean(diff * diff, axis=-1, keepdims=True)
        heads[:, span] = (diff * lax.rsqrt(mean + 1e-06) * gain[...]).astype(BF16)

    for copy in pcopies:
        copy.wait()
    total = proj[0]
    for k in range(1, ntp):
        total = total + proj[k]
    high = total.astype(BF16)
    low = (total - high.astype(F32)).astype(BF16)

    def contract(a, b):
        return lax.dot_general(a, b, (((0,), (0,)), ((), ())), preferred_element_type=F32)

    loads[4].wait()
    rows = vm.shape[0]
    low_v = (contract(high[:, :rank], vcot[...]) + contract(low[:, :rank], vcot[...])) * scale
    part[:, :, :cols] = low_v.astype(BF16).reshape(nfs, rows, cols)
    low_o = (contract(high[:, rank:], heads[...]) + contract(low[:, rank:], heads[...])) * scale
    part[:, :, cols:] = low_o.astype(BF16).reshape(nfs, rows, cols)

    rcopies = []
    for k in range(1, nfs):
        peer = lax.rem(me + k, nfs)
        copy = pltpu.make_async_remote_copy(
            src_ref=part.at[peer], dst_ref=got.at[k],
            send_sem=rsend.at[k], recv_sem=rrecv.at[k],
            device_id={"fs": peer},
        )
        copy.start()
        rcopies.append(copy)

    for s in range(1, nz):
        for kind in ("v", "o"):
            along(kind, s)
        for kind in ("v", "o"):
            if s == 1:
                across(kind, z)
            else:
                behind(kind, s - 1)

    for copy in rcopies:
        copy.wait_recv()
    own = part[me].astype(F32)
    for k in range(1, nfs):
        own = own + got[k].astype(F32)
    own_out[...] = own
    for off, m_ref, s_ref in ((0, vm, vs), (cols, om, os_)):
        g = own[:, off:off + cols]
        m = 0.8 * m_ref[...] + 0.2 * g
        s = 0.95 * s_ref[...] + 0.05 * g * g
        direction[:, off:off + cols] = (m / (jnp.sqrt(s) + 1e-08)).astype(BF16)
    own_d = pltpu.make_async_copy(direction, dfull.at[me], lsem.at[2])
    own_d.start()
    halves = {"dv": direction.at[:, pl.ds(0, cols)], "do": direction.at[:, pl.ds(cols, cols)]}
    for kind, src in halves.items():
        for dz in range(1, nz):
            send(kind, src, me, at(dz, 0, 0))
        spread(kind, src, me)
    for dz in range(1, nz):
        for kind in halves:
            arrived(kind, at(dz, 0, 0))
            spread(kind, None, at(dz, 0, 0))
    for dz in range(nz):
        for kind in halves:
            across(kind, lax.rem(z + dz, nz))
    for kind in ("v", "o"):
        if nz > 1:
            behind(kind, nz - 1)
        else:
            across(kind, z)

    for dz in range(nz):
        for dy in range(ny):
            if nx > 1:
                arrived("v", at(dz, dy, 1))
                arrived("dv", at(dz, dy, 1))
        for dx in range(nx):
            if ny > 1:
                arrived("o", at(dz, 1, dx))
                arrived("do", at(dz, 1, dx))
    for copy in rcopies:
        copy.wait_send()
    for cond, make in pending:
        when(cond, lambda make=make: make().wait_send())
    own_v.wait()
    own_o.wait()
    own_d.wait()


def update(
    width, fs, gv, go, vfac, ofac, dv, do, vw, ow, own, vm, vs, om, os_,
    v_copy, o_copy, v_master, o_master, vm_new, vs_new, om_new, os_new, turned,
):
    step = pl.program_id(0)
    cols = dv.shape[1]

    @pl.when(step == 0)
    def _():
        turned[...] = do[...].T
        for off, m_ref, s_ref, m_out, s_out in (
            (0, vm, vs, vm_new, vs_new),
            (cols, om, os_, om_new, os_new),
        ):
            g = own[:, off:off + cols]
            m_out[...] = 0.8 * m_ref[...] + 0.2 * g
            s_out[...] = 0.95 * s_ref[...] + 0.05 * g * g

    move_v = 0.05 * jnp.dot(vfac[...], dv[...], preferred_element_type=F32)
    move_o = 0.05 * lax.dot_general(
        turned[...], ofac[...], (((1,), (1,)), ((), ())), preferred_element_type=F32
    )
    v_copy[...] = (decode(gv[0]) - move_v).astype(BF16)
    o_old = decode(go[...] if len(go.shape) == 2 else go[0])
    o_new = (o_old - move_o).astype(BF16)
    if len(go.shape) == 2:
        o_copy[...] = o_new
    else:
        o_copy[0] = o_new

    @pl.when(step == fs[0])
    def _():
        v_master[...] = vw[...] - move_v
        o_master[...] = ow[...] - move_o


def local(
    nfs, ntp,
    inputs, value_cotangent, first_map, second_map, lambdas, head_gain,
    output_cotangent, value_factor, output_factor, value_weight, output_weight,
    value_moment, value_second, output_moment, output_second,
):
    tokens, cols = inputs.shape
    width = value_weight.shape[0]
    rank = value_factor.shape[1]
    rows = value_moment.shape[0]
    fs = lax.axis_index("fs")
    scale = 1.0 / math.sqrt(tokens * nfs)
    flat = width % 128 == 0
    go_shape = (cols, nfs * width) if flat else (nfs, cols, width)
    vmem = pl.BlockSpec(memory_space=pltpu.VMEM)
    hbm = pl.BlockSpec(memory_space=pl.ANY)
    dma = pltpu.SemaphoreType.DMA
    moment = jax.ShapeDtypeStruct((rows, cols), F32)
    gv, go, dfull, own = pl.pallas_call(
        functools.partial(exchange, nfs, ntp, scale),
        out_shape=(
            jax.ShapeDtypeStruct((nfs, width, cols), BF16),
            jax.ShapeDtypeStruct(go_shape, BF16),
            jax.ShapeDtypeStruct((nfs, rows, 2 * cols), BF16),
            jax.ShapeDtypeStruct((rows, 2 * cols), F32),
        ),
        in_specs=[vmem] * 2 + [hbm] * 5 + [pl.BlockSpec(memory_space=pltpu.SMEM)] + [vmem] * 7,
        out_specs=(hbm, hbm, hbm, vmem),
        scratch_shapes=[
            pltpu.VMEM((width, cols), BF16),
            pltpu.VMEM((cols, width), BF16),
            *[pltpu.VMEM((tokens, cols), BF16)] * 6,
            pltpu.VMEM((ntp, tokens, 2 * rank), F32),
            pltpu.VMEM((nfs, rows, 2 * cols), BF16),
            pltpu.VMEM((nfs, rows, 2 * cols), BF16),
            pltpu.VMEM((rows, 2 * cols), BF16),
            dma((2 * nfs + 1,)), dma((nfs,)), dma((2 * nfs + 1,)), dma((nfs,)),
            dma((ntp,)), dma((ntp,)),
            dma((nfs,)), dma((nfs,)),
            dma((nfs,)), dma((nfs,)), dma((nfs,)), dma((nfs,)), dma((3,)), dma((5,)),
        ],
        compiler_params=pltpu.CompilerParams(collective_id=0, has_side_effects=True),
    )(
        value_weight, output_weight,
        inputs, output_cotangent, first_map, second_map, value_cotangent,
        lambdas, head_gain.reshape(1, -1), value_factor, output_factor,
        value_moment, value_second, output_moment, output_second,
    )
    dirs = dfull.reshape(nfs * rows, 2 * cols)
    same = lambda i: (0, 0)
    if flat:
        o_spec, oc_shape = pl.BlockSpec((cols, width), lambda i: (0, i)), (cols, nfs * width)
    else:
        o_spec, oc_shape = pl.BlockSpec((1, cols, width), lambda i: (i, 0, 0)), go_shape
    small = pl.BlockSpec((rows, cols), same)
    outs = pl.pallas_call(
        functools.partial(update, width),
        grid=(nfs,),
        out_shape=(
            jax.ShapeDtypeStruct((nfs * width, cols), BF16),
            jax.ShapeDtypeStruct(oc_shape, BF16),
            jax.ShapeDtypeStruct((width, cols), F32),
            jax.ShapeDtypeStruct((cols, width), F32),
            moment, moment, moment, moment,
        ),
        in_specs=[
            pl.BlockSpec(memory_space=pltpu.SMEM),
            pl.BlockSpec((1, width, cols), lambda i: (i, 0, 0)),
            o_spec,
            pl.BlockSpec((width, rank), lambda i: (i, 0)),
            pl.BlockSpec((width, rank), lambda i: (i, 0)),
            pl.BlockSpec((rank, cols), lambda i: (0, 0)),
            pl.BlockSpec((rank, cols), lambda i: (0, 1)),
            pl.BlockSpec((width, cols), same),
            pl.BlockSpec((cols, width), same),
            pl.BlockSpec((rows, 2 * cols), same),
            small, small, small, small,
        ],
        out_specs=(
            pl.BlockSpec((width, cols), lambda i: (i, 0)),
            o_spec,
            pl.BlockSpec((width, cols), same),
            pl.BlockSpec((cols, width), same),
            small, small, small, small,
        ),
        scratch_shapes=[pltpu.VMEM((cols, rank), BF16)],
        compiler_params=pltpu.CompilerParams(dimension_semantics=("arbitrary",)),
    )(
        fs.reshape(1), gv, go, value_factor, output_factor, dirs, dirs,
        value_weight, output_weight, own,
        value_moment, value_second, output_moment, output_second,
    )
    value_copy, output_copy, value_master, output_master, *moments = outs
    if not flat:
        output_copy = output_copy.transpose(1, 0, 2).reshape(cols, nfs * width)
    return (value_master, output_master, *moments, value_copy, output_copy)


def solution(mesh):
    both = P("fs", "tp")
    in_specs = (
        both, both, both, both, P("tp"), P(), both, P(), P(), both, P("tp", "fs"),
        both, both, both, both,
    )
    out_specs = (
        both, P("tp", "fs"), both, both, both, both, P(None, "tp"), P("tp", None),
    )
    body = functools.partial(local, mesh.shape["fs"], mesh.shape["tp"])
    return jax.shard_map(
        body, mesh=mesh, in_specs=in_specs, out_specs=out_specs, check_vma=False
    )
```

profile of v0, /device:TPU:0, one launch (start us, length us, event | category | flops | bytes accessed | tf_op | source)
XLA Modules:
  0.0 118.5 jit_solution(6490754640549243340)
XLA Ops:
  0.6 100.4 %shard_map.206 = (bf16[16,128,1024]{2,1,0:T(8,128)(2,1)}, bf16[1024,2048]{1,0:T(8,128)(2,1)}, bf16[16,16,2048]{2,1,0:T(8,128)(2,1)}, f32[16,2048]{1,0:T(8,128)}) custom-call(f32[128,1024]{1,0:T(8,128)} %vw.1, f32[1024,128]{1,0:T(8,128)} %ow.1, bf16[512,1024]{1,0:T(8,128)(2,1)} %inp_in.1, bf16[512,1024]{1,0:T(8,128)(2,1)} %ocot_in.1, ...), custom_call_target="tpu_custom_call" | custom-call | tf_op jit(solution)/shard_map/pallas_call | solution.py:341
  101.0 17.5 %shard_map.207 = (bf16[2048,1024]{1,0:T(8,128)(2,1)}, bf16[1024,2048]{1,0:T(8,128)(2,1)}, f32[128,1024]{1,0:T(8,128)}, f32[1024,128]{1,0:T(8,128)}, f32[16,1024]...) custom-call(s32[1]{0:T(128)} %bitcast.fs, ...), custom_call_target="tpu_custom_call" | custom-call | tf_op jit(solution)/shard_map/pallas_call | solution.py:378
where the time goes:
time: 119 us
  Pallas kernels  118 us (99%)
    pallas_call x1, Pallas kernels, local(): pl.pallas_call(functools.partial(exchange, nfs, ntp, scale), out_shape=(j...  100 us
    pallas_call x1, Pallas kernels, local(): pl.pallas_call(functools.partial(update, width), grid=(nfs,), out_shape=(...  17.5 us

commit v1 on v0

v1 whole, which is shorter than its diff:
```python
import functools
import math

import jax
import jax.numpy as jnp
from jax import lax
from jax.experimental import pallas as pl
from jax.experimental.pallas import tpu as pltpu
from jax.sharding import PartitionSpec as P

F32 = jnp.float32
BF16 = jnp.bfloat16

CODE = 2.0**30
GRAIN = 2.0**40
NX = 2
NY = 2
NC = NX * NY


def encode(w):
    square = (w * CODE) * (w * CODE)
    fourth = square * square
    return jnp.where(w < 0, -fourth, fourth).astype(BF16)


def decode(v):
    v = v.astype(F32)
    size = lax.rsqrt(lax.rsqrt(jnp.maximum(jnp.abs(v), 1e-36))) * (1.0 / CODE)
    return jnp.where(v < 0, -size, size)


def general(nz):
    js = range(1, nz)
    order = [("zf", "v", 1), ("zf", "v", 2), ("rs1", "v"), ("zf", "o", 1), ("zf", "o", 2), ("nf", "v", 0)]
    order += [("rs1", "o"), ("sp", "v", 1, "y"), ("sp", "v", 1, "x"), ("rs2", "v"), ("nf", "o", 0)]
    order += [("sp", "o", 1, "x"), ("sp", "o", 1, "y"), ("rs2", "o")]
    order += [("zf", kind, j) for j in range(3, nz) for kind in ("v", "o")]
    order += [("agz", "v", j) for j in js] + [("agz", "o", j) for j in js]
    order += [("dg", "v"), ("dg", "o")]
    order += [("sp", "v", 2, "y"), ("sp", "v", 2, "x"), ("sp", "o", 2, "x"), ("sp", "o", 2, "y")]
    order += [("agn", kind, j) for kind in ("v", "o") for j in range(nz)]
    order += [("nf", "v", 1), ("nf", "o", 1)]
    for j in range(3, nz):
        order += [("sp", "v", j, "y"), ("sp", "v", j, "x"), ("sp", "o", j, "x"), ("sp", "o", j, "y")]
    order += [("dz", kind, j) for j in (1, 2) for kind in ("v", "o")]
    for kind in ("v", "o"):
        order += [("dirs", kind), ("up", kind, 0, "c"), ("up", kind, 0, "d"), ("nf", kind, 2)]
    order += [("dz", kind, j) for j in range(3, nz) for kind in ("v", "o")]
    for j in js:
        order += [("nf", kind, j) for kind in ("v", "o") if j >= 3]
        order += [("up", kind, j, part) for kind in ("v", "o") for part in ("c", "d")]
    return [
        ("a", "v", "z"), ("a", "o", "z"), ("a", "v", "y"), ("a", "v", "x"),
        ("c", "v"), ("c", "o"), ("a", "o", "x"), ("a", "o", "y"),
    ] + [step for step in order if len(step) < 3 or step[2] < nz]


def squared(g):
    g = g * GRAIN
    return (g * jnp.abs(g)).astype(BF16)


def rooted(v):
    v = v.astype(F32)
    return v * lax.rsqrt(jnp.maximum(jnp.abs(v), 1e-36)) * (1.0 / GRAIN)


def schedule(nz):
    return general(nz)


def exchange(
    nfs, ntp, scale,
    vw_hbm, ow_hbm, inp_hbm, vfac_hbm, ocot_hbm, ofac_hbm, vcot_hbm, first_hbm, second_hbm,
    vm_hbm, vs_hbm, om_hbm, os_hbm, lam_hbm, gain_hbm,
    v_out, o_out, v_master, o_master, vm_new, vs_new, om_new, os_new,
    vw_in, ow_in, inp, vfac, ocot, ofac, vcot, first, second, vm, vs, om, os_, lam, gain,
    gv, go, heads, proj_v, proj_o,
    part_v, part_o, got_v, got_o, sum_v, sum_o, col_v, col_o,
    dfull_v, dfull_o, turned,
    wsend, wrecv, drecv, psend, precv, rsend, rrecv, csend, crecv, asend, arecv, insem,
):
    me = lax.axis_index("fs")
    tp = lax.axis_index("tp")
    tokens, cols = inp.shape
    width = vw_in.shape[0]
    rows = vm.shape[0]
    nz = nfs // NC
    x = lax.rem(me, NX)
    y = lax.rem(lax.div(me, NX), NY)
    z = lax.div(me, NC)
    ox, oy = 1 - x, 1 - y
    cut = {"v": width * 7 // 8 // 16 * 16, "o": cols * 7 // 8 // 16 * 16}
    size = {"v": width, "o": cols}
    index = {"v": 0, "o": 1}
    store = {"v": gv, "o": go}
    flat = len(o_out.shape) == 2

    def at(p, cy, cx):
        return (p * NY + cy) * NX + cx

    below = nz - 1 - z
    pairs = jnp.minimum(z, below)

    def plane(j):
        if j == 0:
            return z
        near = z + (-1 if j % 2 else 1) * ((j + 1) // 2)
        rest = jnp.where(z < below, j, nz - 1 - j)
        return jnp.where(j <= 2 * pairs, near, rest)

    planes = [plane(j) for j in range(nz)]

    def onward(j):
        p = planes[j]
        rising = p < z
        go_on = (rising & (z + 1 < nz)) | (jnp.logical_not(rising) & (z > 0))
        target = at(jnp.where(rising, lax.rem(z + 1, nz), lax.rem(z + nz - 1, nz)), y, x)
        return go_on, target

    barrier = pltpu.get_barrier_semaphore()
    for k in (1, 2, 3):
        pl.semaphore_signal(barrier, inc=1, device_id={"fs": at(z, oy if k & 2 else y, ox if k & 1 else x)})
    for k in range(1, nz):
        pl.semaphore_signal(barrier, inc=1, device_id={"fs": at(lax.rem(z + k, nz), y, x)})
    for k in range(1, ntp):
        pl.semaphore_signal(barrier, inc=1, device_id={"tp": lax.rem(tp + k, ntp)})
    loads = {}
    inputs = {
        "vw": (vw_hbm, vw_in), "ow": (ow_hbm, ow_in), "inp": (inp_hbm, inp), "vfac": (vfac_hbm, vfac),
        "ocot": (ocot_hbm, ocot), "ofac": (ofac_hbm, ofac), "vcot": (vcot_hbm, vcot),
        "first": (first_hbm, first), "second": (second_hbm, second),
        "vm": (vm_hbm, vm), "vs": (vs_hbm, vs), "om": (om_hbm, om), "os": (os_hbm, os_),
        "lam": (lam_hbm, lam), "gain": (gain_hbm, gain),
    }
    for k, (name, (src, dst)) in enumerate(inputs.items()):
        loads[name] = pltpu.make_async_copy(src, dst, insem.at[k])
        loads[name].start()
    loads["vw"].wait()
    gv[me] = encode(vw_in[...])
    loads["ow"].wait()
    go[me] = encode(ow_in[...])
    pl.semaphore_wait(barrier, NC + nz + ntp - 3)

    pending = []
    counts = {}

    def when(cond, run):
        if cond is None:
            run()
        else:
            pl.when(cond)(run)

    def send(sems, kind, src, dst, recv, target, cond=None):
        k = counts.get((id(sems), kind), 0)
        counts[(id(sems), kind)] = k + 1

        def make():
            return pltpu.make_async_remote_copy(
                src_ref=src, dst_ref=dst, send_sem=sems.at[index[kind], k],
                recv_sem=recv, device_id={"fs": target},
            )

        when(cond, lambda: make().start())
        pending.append((cond, make))

    def landed(ref, recv, cond=None):
        when(cond, lambda: pltpu.make_async_remote_copy(
            src_ref=ref, dst_ref=ref, send_sem=wsend.at[0, 0], recv_sem=recv,
            device_id={"fs": at(z, y, ox)},
        ).wait_recv())

    def block(kind, b, part=None):
        ref = store[kind].at[b]
        if part is None:
            return ref, wrecv.at[index[kind], b]
        if part == 0:
            return store[kind].at[b, pl.ds(0, cut[kind])], drecv.at[index[kind], b]
        rest = size[kind] - cut[kind]
        return store[kind].at[b, pl.ds(cut[kind], rest)], wrecv.at[index[kind], b]

    def push(kind, b, target, part=None, cond=None):
        ref, recv = block(kind, b, part)
        send(wsend, kind, ref, ref, recv, target, cond)

    def arrived(kind, b, part=None, cond=None):
        ref, recv = block(kind, b, part)
        landed(ref, recv, cond)

    to_x, to_y = at(z, y, ox), at(z, oy, x)
    up, down = at(lax.rem(z + 1, nz), y, x), at(lax.rem(z + nz - 1, nz), y, x)

    links = {"x": to_x, "y": to_y}

    def own_send(kind, link):
        if link == "z":
            push(kind, me, up, cond=z + 1 < nz)
            push(kind, me, down, cond=z > 0)
        else:
            push(kind, me, links[link])

    mine = pl.ds(pl.multiple_of(tp * cols, cols), cols)
    pcopies = {}

    def project(kind, cot, factor, proj):
        proj[0] = jnp.dot(cot[...], factor[mine, :], preferred_element_type=F32)
        pcopies[kind] = []
        for k in range(1, ntp):
            copy = pltpu.make_async_remote_copy(
                src_ref=proj.at[0], dst_ref=proj.at[k],
                send_sem=psend.at[index[kind], k], recv_sem=precv.at[index[kind], k],
                device_id={"tp": lax.rem(tp + k, ntp)},
            )
            copy.start()
            pcopies[kind].append(copy)

    def contract(a, b):
        return lax.dot_general(a, b, (((0,), (0,)), ((), ())), preferred_element_type=F32)

    def reduce_low(kind, proj, right, part, got):
        for copy in pcopies[kind]:
            copy.wait()
        total = proj[0]
        for k in range(1, ntp):
            total = total + proj[k]
        high = total.astype(BF16)
        low = (total - high.astype(F32)).astype(BF16)
        product = (contract(high, right[...]) + contract(low, right[...])) * scale
        for b in range(nfs):
            part[b % NC, b // NC] = squared(product[b * rows:(b + 1) * rows])
        for k in (1, 2, 3):
            cx = ox if k & 1 else x
            cy = oy if k & 2 else y
            send(rsend, kind, part.at[cy * NX + cx], got.at[k], rrecv.at[index[kind], k], at(z, cy, cx))

    def fetch(*names):
        for name in names:
            loads[name].wait()

    def normalize():
        head_width = gain.shape[1]
        for h in range(cols // head_width):
            span = pl.ds(h * head_width, head_width)
            diff = first[:, span].astype(F32) - lam[h] * second[:, span].astype(F32)
            mean = jnp.mean(diff * diff, axis=-1, keepdims=True)
            heads[:, span] = (diff * lax.rsqrt(mean + 1e-06) * gain[...]).astype(BF16)

    def compute(kind):
        if kind == "v":
            fetch("inp", "vfac")
            project("v", inp, vfac, proj_v)
            fetch("ocot", "ofac")
            project("o", ocot, ofac, proj_o)
            fetch("vcot")
            reduce_low("v", proj_v, vcot, part_v, got_v)
        else:
            fetch("first", "second", "lam", "gain", "vm", "vs", "om", "os")
            normalize()
            reduce_low("o", proj_o, heads, part_o, got_o)

    parts = {"v": (part_v, got_v, sum_v, col_v), "o": (part_o, got_o, sum_o, col_o)}
    moments = {"v": (vm, vs, vm_new, vs_new), "o": (om, os_, om_new, os_new)}
    dfull = {"v": dfull_v, "o": dfull_o}

    def rs1(kind):
        part, got, total, col = parts[kind]
        for k in (1, 2, 3):
            landed(got.at[k], rrecv.at[index[kind], k])
        acc = rooted(part[y * NX + x])
        for k in (1, 2, 3):
            acc = acc + rooted(got[k])
        total[...] = squared(acc)
        for d in range(1, nz):
            peer = lax.rem(z + d, nz)
            send(csend, kind, total.at[peer], col.at[d], crecv.at[index[kind], d], at(peer, y, x))

    def rs2(kind):
        part, got, total, col = parts[kind]
        m_ref, s_ref, m_out, s_out = moments[kind]
        for d in range(1, nz):
            landed(col.at[d], crecv.at[index[kind], d])
        g = rooted(total[z])
        for d in range(1, nz):
            g = g + rooted(col[d])
        m = 0.8 * m_ref[...] + 0.2 * g
        s = 0.95 * s_ref[...] + 0.05 * g * g
        m_out[...] = m
        s_out[...] = s
        dfull[kind][me] = (m / (jnp.sqrt(s) + 1e-08)).astype(BF16)
        for d in range(1, nz):
            apush(kind, me, at(lax.rem(z + d, nz), y, x))
        aspread(kind, me)

    def apush(kind, b, target):
        ref = dfull[kind].at[b]
        send(asend, kind, ref, ref, arecv.at[index[kind], b], target)

    def aspread(kind, b):
        for target in (to_y, to_x) if kind == "v" else (to_x, to_y):
            apush(kind, b, target)

    def alanded(kind, b):
        landed(dfull[kind].at[b], arecv.at[index[kind], b])

    def agz(kind, j):
        b = at(planes[j], y, x)
        alanded(kind, b)
        aspread(kind, b)

    def agn(kind, j):
        b = at(planes[j], oy, x) if kind == "v" else at(planes[j], y, ox)
        alanded(kind, b)
        apush(kind, b, to_x if kind == "v" else to_y)

    def whole(kind):
        d = dfull[kind][...]
        if rows % 16:
            return d.astype(F32).reshape(nfs * rows, cols).astype(BF16)
        return d.reshape(nfs * rows, cols)

    def dirs(kind):
        for p in planes:
            alanded(kind, at(p, y, ox) if kind == "v" else at(p, oy, x))
            alanded(kind, at(p, oy, ox))
        if kind == "o":
            turned[...] = whole(kind).T

    def factor_rows(b, r0, n):
        return pl.ds(pl.multiple_of(b * width + r0, 16), n)

    def move_v(b, r0, n):
        return 0.05 * jnp.dot(vfac[factor_rows(b, r0, n), :], whole("v"), preferred_element_type=F32)

    def move_o(b, r0, n):
        return 0.05 * lax.dot_general(
            turned[pl.ds(r0, n), :], ofac[factor_rows(b, 0, width), :],
            (((1,), (1,)), ((), ())), preferred_element_type=F32,
        )

    def put_o(b, r0, n, new):
        if flat:
            o_out[pl.ds(r0, n), pl.ds(pl.multiple_of(b * width, width), width)] = new
        else:
            o_out[b, pl.ds(r0, n), :] = new

    def refresh(kind, b, r0=0, n=None):
        n = size[kind] - r0 if n is None else n
        if kind == "v":
            old = decode(gv[b, pl.ds(r0, n), :])
            v_out[factor_rows(b, r0, n), :] = (old - move_v(b, r0, n)).astype(BF16)
        else:
            old = decode(go[b, pl.ds(r0, n), :])
            put_o(b, r0, n, (old - move_o(b, r0, n)).astype(BF16))

    def own(kind):
        if kind == "v":
            new = vw_in[...] - move_v(me, 0, width)
            v_master[...] = new
            v_out[factor_rows(me, 0, width), :] = new.astype(BF16)
        else:
            new = ow_in[...] - move_o(me, 0, cols)
            o_master[...] = new
            put_o(me, 0, cols, new.astype(BF16))

    waited = {}

    def await_block(what, kind, j, cond=None):
        p = planes[j]
        b, part = {
            "a": (at(p, y, x), None),
            "n": (at(p, oy, x) if kind == "v" else at(p, y, ox), None),
            "m": (at(p, y, ox) if kind == "v" else at(p, oy, x), None),
            "d": (at(p, oy, ox), 1 if j else None),
            "e": (at(p, oy, ox), 0),
        }[what]
        state = waited.get((what, kind, j))
        if state == "all" or (state == "some" and cond is not None):
            return b
        if state == "some":
            arrived(kind, b, part, jnp.logical_not(onward(j)[0]))
        else:
            arrived(kind, b, part, cond)
        waited[what, kind, j] = "all" if cond is None else "some"
        return b

    def zf(kind, j):
        go_on, target = onward(j)
        push(kind, await_block("a", kind, j, go_on), target, cond=go_on)

    def sp(kind, j, link):
        push(kind, await_block("a", kind, j), links[link])

    def nf(kind, j):
        push(kind, await_block("n", kind, j), to_x if kind == "v" else to_y, 1 if j else None)

    def dg(kind):
        b = await_block("d", kind, 0)
        push(kind, b, up, 0, z + 1 < nz)
        push(kind, b, down, 0, z > 0)

    def dz(kind, j):
        go_on, target = onward(j)
        push(kind, await_block("e", kind, j, go_on), target, 0, go_on)

    def update(kind, j, part):
        p = planes[j]
        if part == "d":
            b = await_block("d", kind, j)
            if j:
                await_block("e", kind, j)
            refresh(kind, b)
            return
        if j:
            await_block("a", kind, j)
        await_block("n", kind, j)
        await_block("m", kind, j)
        if j == 0:
            own(kind)

        def step(c, carry):
            cy = jnp.where(c == 2, oy, y)
            cx = jnp.where(c == 1, ox, x)
            refresh(kind, at(p, cy, cx))
            return carry

        lax.fori_loop(0 if j else 1, 3, step, 0)

    ops = {
        "a": own_send, "c": compute, "zf": zf, "sp": sp, "nf": nf, "dg": dg, "dz": dz,
        "rs1": rs1, "rs2": rs2, "agz": agz, "agn": agn, "dirs": dirs, "up": update,
    }
    for name, *args in schedule(nz):
        ops[name](*args)
    for cond, make in pending:
        when(cond, lambda make=make: make().wait_send())


def publish(count, *refs):
    sems = refs[-1]
    copies = [
        pltpu.make_async_copy(refs[k], refs[count + k], sems.at[k]) for k in range(count)
    ]
    for copy in copies:
        copy.start()
    for copy in copies:
        copy.wait()


def local(
    nfs, ntp,
    inputs, value_cotangent, first_map, second_map, lambdas, head_gain,
    output_cotangent, value_factor, output_factor, value_weight, output_weight,
    value_moment, value_second, output_moment, output_second,
):
    tokens, cols = inputs.shape
    width = value_weight.shape[0]
    rank = value_factor.shape[1]
    rows = value_moment.shape[0]
    nz = nfs // NC
    scale = 1.0 / math.sqrt(tokens * nfs)
    flat = width % 128 == 0
    vmem = pl.BlockSpec(memory_space=pltpu.VMEM)
    hbm = pl.BlockSpec(memory_space=pl.ANY)
    dma = pltpu.SemaphoreType.DMA
    moment = jax.ShapeDtypeStruct((rows, cols), F32)
    out_shape = (
        jax.ShapeDtypeStruct((nfs * width, cols), BF16),
        jax.ShapeDtypeStruct((cols, nfs * width) if flat else (nfs, cols, width), BF16),
        jax.ShapeDtypeStruct((width, cols), F32),
        jax.ShapeDtypeStruct((cols, width), F32),
        moment, moment, moment, moment,
    )
    operands = (
        value_weight, output_weight, inputs, value_factor, output_cotangent, output_factor,
        value_cotangent, first_map, second_map,
        value_moment, value_second, output_moment, output_second, lambdas, head_gain.reshape(1, -1),
    )
    spaces = [pltpu.SMEM if operand is lambdas else pltpu.VMEM for operand in operands]
    shapes = [
        ((nfs, width, cols), BF16),
        ((nfs, cols, width), BF16),
        ((tokens, cols), BF16),
        *[((ntp, tokens, rank), F32)] * 2,
        *[((NC, nz, rows, cols), BF16)] * 4,
        *[((nz, rows, cols), BF16)] * 4,
        *[((nfs, rows, cols), BF16)] * 2,
        ((cols, rank), BF16),
    ]
    sends = 4 + 9 * nz
    outs = pl.pallas_call(
        functools.partial(exchange, nfs, ntp, scale),
        out_shape=tuple(pltpu.VMEM(out.shape, out.dtype) for out in out_shape),
        in_specs=[hbm] * len(operands),
        out_specs=(vmem,) * 8,
        scratch_shapes=[
            *[space(operand.shape, operand.dtype) for space, operand in zip(spaces, operands)],
            *[pltpu.VMEM(shape, dtype) for shape, dtype in shapes],
            dma((2, sends)), dma((2, nfs)), dma((2, nfs)),
            dma((2, ntp)), dma((2, ntp)),
            dma((2, NC)), dma((2, NC)),
            dma((2, nz)), dma((2, nz)),
            dma((2, 5 * nz)), dma((2, nfs)), dma((len(operands),)),
        ],
        compiler_params=pltpu.CompilerParams(collective_id=0, has_side_effects=True, vmem_limit_bytes=VMEM_LIMIT),
    )(
        *[pltpu.with_memory_space_constraint(operand, pltpu.HBM) for operand in operands],
    )
    outs = pl.pallas_call(
        functools.partial(publish, len(outs)),
        out_shape=out_shape,
        in_specs=[vmem] * len(outs),
        out_specs=(hbm,) * len(outs),
        scratch_shapes=[dma((len(outs),))],
        compiler_params=pltpu.CompilerParams(vmem_limit_bytes=VMEM_LIMIT),
    )(*outs)
    value_copy, output_copy, value_master, output_master, *moments = outs
    if not flat:
        output_copy = output_copy.transpose(1, 0, 2).reshape(cols, nfs * width)
    return (value_master, output_master, *moments, value_copy, output_copy)


VMEM_LIMIT = 40 * 1024 * 1024


def solution(mesh):
    both = P("fs", "tp")
    in_specs = (
        both, both, both, both, P("tp"), P(), both, P(), P(), both, P("tp", "fs"),
        both, both, both, both,
    )
    out_specs = (
        both, P("tp", "fs"), both, both, both, both, P(None, "tp"), P("tp", None),
    )
    body = functools.partial(local, mesh.shape["fs"], mesh.shape["tp"])
    return jax.shard_map(
        body, mesh=mesh, in_specs=in_specs, out_specs=out_specs, check_vma=False
    )
```

time: 119 us -> 91.4 us (0.77)
  Pallas kernels: 118 us -> 90.6 us
    pallas_call x2, Pallas kernels: 118 us -> 90.6 us  [the longest x1 86.9 us: local(): pl.pallas_call(functools.partial(exchange, nfs, ntp, scale), out_shape=tu...]
where the time goes in v1:
time: 91.4 us; the launch traced here: 91.2 us
  Pallas kernels  90.6 us (99%)
    pallas_call x1, Pallas kernels, local(): pl.pallas_call(functools.partial(exchange, nfs, ntp, scale), out_shape=tu...  86.9 us
    pallas_call x1, Pallas kernels, local(): pl.pallas_call(functools.partial(publish, len(outs)), out_shape=out_shape...  3.72 us

profile of v1, /device:TPU:0, one launch (start us, length us, event | category | flops | bytes accessed | tf_op | source)
XLA Modules:
  0.0 91.2 jit_solution(11037715035689699057)
XLA Ops:
  0.6 86.9 %shard_map.206 = (bf16[2048,1024]{1,0:T(8,128)(2,1)S(1)}, bf16[1024,2048]{1,0:T(8,128)(2,1)S(1)}, f32[128,1024]{1,0:T(8,128)S(1)}, f32[1024,128]{1,0:T(8,128)S(1...) custom-call(f32[128,1024]{1,0:T(8,128)} %vw_hbm.1, ...), custom_call_target="tpu_custom_call" | custom-call | tf_op jit(solution)/shard_map/pallas_call | solution.py:491
  87.5 3.7 %shard_map.207 = (bf16[2048,1024]{1,0:T(8,128)(2,1)}, bf16[1024,2048]{1,0:T(8,128)(2,1)}, f32[128,1024]{1,0:T(8,128)}, f32[1024,128]{1,0:T(8,128)}, f32[16,1024]...) custom-call(bf16[2048,1024]{1,0:T(8,128)(2,1)S(1)} %get-tuple-element.24.refs_0_, ...), custom_call_target="tpu_custom_call" | custom-call | tf_op jit(solution)/shard_map/pallas_call | solution.py:509

commit v2 on v1

--- a/solution.py
+++ b/solution.py
@@ -66,8 +66,26 @@
     return v * lax.rsqrt(jnp.maximum(jnp.abs(v), 1e-36)) * (1.0 / GRAIN)
 
 
+STEPS = (
+    ("a", "v", "x"), ("a", "o", "z"), ("a", "v", "y"), ("a", "v", "z"), ("c", "v"), ("zf", "o", 2),
+    ("zf", "o", 1), ("a", "o", "x"), ("sp", "v", 1, "y"), ("rs1", "v"), ("c", "o"), ("sp", "o", 1, "x"),
+    ("sp", "o", 2, "y"), ("nf", "v", 0), ("zf", "v", 1), ("rs2", "v"), ("zf", "v", 2), ("rs1", "o"),
+    ("agz", "v", 1), ("sp", "v", 2, "y"), ("agz", "v", 2), ("nf", "o", 0), ("rs2", "o"), ("zf", "v", 3),
+    ("dg", "v"), ("agz", "v", 3), ("agz", "o", 1), ("zf", "o", 3), ("a", "o", "y"), ("agn", "o", 0),
+    ("sp", "o", 2, "x"), ("nf", "v", 1), ("agz", "o", 2), ("nf", "v", 2), ("agz", "o", 3), ("agn", "v", 1),
+    ("dz", "v", 1), ("nf", "o", 2), ("agn", "v", 3), ("agn", "o", 1), ("nf", "o", 1), ("agn", "v", 0),
+    ("agn", "v", 2), ("dg", "o"), ("sp", "v", 2, "x"), ("dirs", "v"), ("dz", "v", 2), ("agn", "o", 3),
+    ("agn", "o", 2), ("up", "v", 0, "c"), ("sp", "o", 1, "y"), ("sp", "o", 3, "x"), ("dirs", "o"),
+    ("up", "o", 0, "d"), ("sp", "v", 1, "x"), ("sp", "v", 3, "y"), ("up", "o", 1, "d"), ("up", "v", 1, "d"),
+    ("dz", "o", 1), ("dz", "o", 2), ("up", "v", 2, "d"), ("up", "v", 2, "c"), ("up", "o", 2, "c"),
+    ("nf", "o", 3), ("sp", "o", 3, "y"), ("up", "o", 2, "d"), ("dz", "o", 3), ("dz", "v", 3),
+    ("up", "o", 1, "c"), ("sp", "v", 3, "x"), ("up", "v", 0, "d"), ("nf", "v", 3), ("up", "o", 0, "c"),
+    ("up", "v", 1, "c"), ("up", "o", 3, "d"), ("up", "o", 3, "c"), ("up", "v", 3, "c"), ("up", "v", 3, "d"),
+)
+
+
 def schedule(nz):
-    return general(nz)
+    return STEPS if nz == 4 else general(nz)
 
 
 def exchange(
@@ -79,7 +97,7 @@
     gv, go, heads, proj_v, proj_o,
     part_v, part_o, got_v, got_o, sum_v, sum_o, col_v, col_o,
     dfull_v, dfull_o, turned,
-    wsend, wrecv, drecv, psend, precv, rsend, rrecv, csend, crecv, asend, arecv, insem,
+    wsend, wrecv, drecv, psend, precv, rsend, rrecv, csend, crecv, asend, arecv, insem, rising, falling, corner,
 ):
     me = lax.axis_index("fs")
     tp = lax.axis_index("tp")
@@ -97,6 +115,12 @@
     store = {"v": gv, "o": go}
     flat = len(o_out.shape) == 2
 
+    def when(cond, run):
+        if cond is None:
+            run()
+        else:
+            pl.when(cond)(run)
+
     def at(p, cy, cx):
         return (p * NY + cy) * NX + cx
 
@@ -119,11 +143,12 @@
         target = at(jnp.where(rising, lax.rem(z + 1, nz), lax.rem(z + nz - 1, nz)), y, x)
         return go_on, target
 
+    to_x, to_y = at(z, y, ox), at(z, oy, x)
+    up, down = at(lax.rem(z + 1, nz), y, x), at(lax.rem(z + nz - 1, nz), y, x)
+    has_up, has_down = z + 1 < nz, z > 0
     barrier = pltpu.get_barrier_semaphore()
-    for k in (1, 2, 3):
-        pl.semaphore_signal(barrier, inc=1, device_id={"fs": at(z, oy if k & 2 else y, ox if k & 1 else x)})
-    for k in range(1, nz):
-        pl.semaphore_signal(barrier, inc=1, device_id={"fs": at(lax.rem(z + k, nz), y, x)})
+    for target, cond in ((to_x, None), (to_y, None), (up, has_up), (down, has_down)):
+        when(cond, lambda target=target: pl.semaphore_signal(barrier, inc=1, device_id={"fs": target}))
     for k in range(1, ntp):
         pl.semaphore_signal(barrier, inc=1, device_id={"tp": lax.rem(tp + k, ntp)})
     loads = {}
@@ -136,21 +161,33 @@
     }
     for k, (name, (src, dst)) in enumerate(inputs.items()):
         loads[name] = pltpu.make_async_copy(src, dst, insem.at[k])
+    first_loads = ("vw", "ow", "inp", "vfac")
+    for name in first_loads:
         loads[name].start()
     loads["vw"].wait()
+    for name in loads:
+        if name not in first_loads:
+            loads[name].start()
     gv[me] = encode(vw_in[...])
     loads["ow"].wait()
     go[me] = encode(ow_in[...])
-    pl.semaphore_wait(barrier, NC + nz + ntp - 3)
+    pl.semaphore_wait(barrier, 1 + ntp + jnp.where(has_up, 1, 0) + jnp.where(has_down, 1, 0))
+
+    def tell(k):
+        when(has_up, lambda: pl.semaphore_signal(rising.at[k], inc=1, device_id={"fs": up}))
+        when(has_down, lambda: pl.semaphore_signal(falling.at[k], inc=1, device_id={"fs": down}))
+
+    def hear(k):
+        when(has_down, lambda: pl.semaphore_wait(rising.at[k], 1))
+        when(has_up, lambda: pl.semaphore_wait(falling.at[k], 1))
+
+    pl.semaphore_signal(corner, inc=1, device_id={"fs": to_x})
+    steps = max(nz - 2, 0)
+    if steps:
+        tell(0)
 
     pending = []
     counts = {}
-
-    def when(cond, run):
-        if cond is None:
-            run()
-        else:
-            pl.when(cond)(run)
 
     def send(sems, kind, src, dst, recv, target, cond=None):
         k = counts.get((id(sems), kind), 0)
@@ -195,8 +232,8 @@
 
     def own_send(kind, link):
         if link == "z":
-            push(kind, me, up, cond=z + 1 < nz)
-            push(kind, me, down, cond=z > 0)
+            push(kind, me, up, cond=has_up)
+            push(kind, me, down, cond=has_down)
         else:
             push(kind, me, links[link])
 
@@ -253,6 +290,10 @@
             fetch("ocot", "ofac")
             project("o", ocot, ofac, proj_o)
             fetch("vcot")
+            pl.semaphore_wait(corner, 1)
+            for k in range(1, steps):
+                hear(k - 1)
+                tell(k)
             reduce_low("v", proj_v, vcot, part_v, got_v)
         else:
             fetch("first", "second", "lam", "gain", "vm", "vs", "om", "os")
@@ -263,8 +304,13 @@
     moments = {"v": (vm, vs, vm_new, vs_new), "o": (om, os_, om_new, os_new)}
     dfull = {"v": dfull_v, "o": dfull_o}
 
+    heard = []
+
     def rs1(kind):
         part, got, total, col = parts[kind]
+        if steps and not heard:
+            hear(steps - 1)
+            heard.append(True)
         for k in (1, 2, 3):
             landed(got.at[k], rrecv.at[index[kind], k])
         acc = rooted(part[y * NX + x])
@@ -396,8 +442,8 @@
 
     def dg(kind):
         b = await_block("d", kind, 0)
-        push(kind, b, up, 0, z + 1 < nz)
-        push(kind, b, down, 0, z > 0)
+        push(kind, b, up, 0, has_up)
+        push(kind, b, down, 0, has_down)
 
     def dz(kind, j):
         go_on, target = onward(j)
@@ -463,6 +509,7 @@
     vmem = pl.BlockSpec(memory_space=pltpu.VMEM)
     hbm = pl.BlockSpec(memory_space=pl.ANY)
     dma = pltpu.SemaphoreType.DMA
+    regular = pltpu.SemaphoreType.REGULAR
     moment = jax.ShapeDtypeStruct((rows, cols), F32)
     out_shape = (
         jax.ShapeDtypeStruct((nfs * width, cols), BF16),
@@ -501,6 +548,7 @@
             dma((2, NC)), dma((2, NC)),
             dma((2, nz)), dma((2, nz)),
             dma((2, 5 * nz)), dma((2, nfs)), dma((len(operands),)),
+            regular((max(nz - 2, 1),)), regular((max(nz - 2, 1),)), regular,
         ],
         compiler_params=pltpu.CompilerParams(collective_id=0, has_side_effects=True, vmem_limit_bytes=VMEM_LIMIT),
     )(

time: 91.4 us -> 88.4 us (0.967)
  Pallas kernels: 90.6 us -> 87.6 us
    pallas_call x1, Pallas kernels: 86.9 us -> 83.9 us  [local(): pl.pallas_call(functools.partial(exchange, nfs, ntp, scale), out_shape=tu...]
where the time goes in v2:
time: 88.4 us; the launch traced here: 88.3 us
  Pallas kernels  87.6 us (99%)
    pallas_call x1, Pallas kernels, local(): pl.pallas_call(functools.partial(exchange, nfs, ntp, scale), out_shape=tu...  83.9 us
    pallas_call x1, Pallas kernels, local(): pl.pallas_call(functools.partial(publish, len(outs)), out_shape=out_shape...  3.72 us

profile of v2, /device:TPU:0, one launch (start us, length us, event | category | flops | bytes accessed | tf_op | source)
XLA Modules:
  0.0 88.3 jit_solution(18059648450273906799)
XLA Ops:
  0.6 83.9 %shard_map.206 = (bf16[2048,1024]{1,0:T(8,128)(2,1)S(1)}, bf16[1024,2048]{1,0:T(8,128)(2,1)S(1)}, f32[128,1024]{1,0:T(8,128)S(1)}, f32[1024,128]{1,0:T(8,128)S(1...) custom-call(f32[128,1024]{1,0:T(8,128)} %vw_hbm.1, ...), custom_call_target="tpu_custom_call" | custom-call | tf_op jit(solution)/shard_map/pallas_call | solution.py:538
  84.6 3.7 %shard_map.207 = (bf16[2048,1024]{1,0:T(8,128)(2,1)}, bf16[1024,2048]{1,0:T(8,128)(2,1)}, f32[128,1024]{1,0:T(8,128)}, f32[1024,128]{1,0:T(8,128)}, f32[16,1024]...) custom-call(bf16[2048,1024]{1,0:T(8,128)(2,1)S(1)} %get-tuple-element.24.refs_0_, ...), custom_call_target="tpu_custom_call" | custom-call | tf_op jit(solution)/shard_map/pallas_call | solution.py:557

commit v3 on v2

--- a/solution.py
+++ b/solution.py
@@ -32,8 +32,8 @@
 
 def general(nz):
     js = range(1, nz)
-    order = [("zf", "v", 1), ("zf", "v", 2), ("rs1", "v"), ("zf", "o", 1), ("zf", "o", 2), ("nf", "v", 0)]
-    order += [("rs1", "o"), ("sp", "v", 1, "y"), ("sp", "v", 1, "x"), ("rs2", "v"), ("nf", "o", 0)]
+    order = [("zf", "v", 1), ("zf", "v", 2), ("ra", "v"), ("rs1", "v"), ("zf", "o", 1), ("zf", "o", 2), ("nf", "v", 0)]
+    order += [("ra", "o"), ("rs1", "o"), ("sp", "v", 1, "y"), ("sp", "v", 1, "x"), ("rs2", "v"), ("nf", "o", 0)]
     order += [("sp", "o", 1, "x"), ("sp", "o", 1, "y"), ("rs2", "o")]
     order += [("zf", kind, j) for j in range(3, nz) for kind in ("v", "o")]
     order += [("agz", "v", j) for j in js] + [("agz", "o", j) for j in js]
@@ -67,20 +67,21 @@
 
 
 STEPS = (
-    ("a", "v", "x"), ("a", "o", "z"), ("a", "v", "y"), ("a", "v", "z"), ("c", "v"), ("zf", "o", 2),
-    ("zf", "o", 1), ("a", "o", "x"), ("sp", "v", 1, "y"), ("rs1", "v"), ("c", "o"), ("sp", "o", 1, "x"),
-    ("sp", "o", 2, "y"), ("nf", "v", 0), ("zf", "v", 1), ("rs2", "v"), ("zf", "v", 2), ("rs1", "o"),
-    ("agz", "v", 1), ("sp", "v", 2, "y"), ("agz", "v", 2), ("nf", "o", 0), ("rs2", "o"), ("zf", "v", 3),
-    ("dg", "v"), ("agz", "v", 3), ("agz", "o", 1), ("zf", "o", 3), ("a", "o", "y"), ("agn", "o", 0),
-    ("sp", "o", 2, "x"), ("nf", "v", 1), ("agz", "o", 2), ("nf", "v", 2), ("agz", "o", 3), ("agn", "v", 1),
-    ("dz", "v", 1), ("nf", "o", 2), ("agn", "v", 3), ("agn", "o", 1), ("nf", "o", 1), ("agn", "v", 0),
-    ("agn", "v", 2), ("dg", "o"), ("sp", "v", 2, "x"), ("dirs", "v"), ("dz", "v", 2), ("agn", "o", 3),
-    ("agn", "o", 2), ("up", "v", 0, "c"), ("sp", "o", 1, "y"), ("sp", "o", 3, "x"), ("dirs", "o"),
-    ("up", "o", 0, "d"), ("sp", "v", 1, "x"), ("sp", "v", 3, "y"), ("up", "o", 1, "d"), ("up", "v", 1, "d"),
-    ("dz", "o", 1), ("dz", "o", 2), ("up", "v", 2, "d"), ("up", "v", 2, "c"), ("up", "o", 2, "c"),
-    ("nf", "o", 3), ("sp", "o", 3, "y"), ("up", "o", 2, "d"), ("dz", "o", 3), ("dz", "v", 3),
-    ("up", "o", 1, "c"), ("sp", "v", 3, "x"), ("up", "v", 0, "d"), ("nf", "v", 3), ("up", "o", 0, "c"),
-    ("up", "v", 1, "c"), ("up", "o", 3, "d"), ("up", "o", 3, "c"), ("up", "v", 3, "c"), ("up", "v", 3, "d"),
+    ("a", "v", "y"), ("a", "o", "z"), ("a", "o", "x"), ("c", "v"), ("a", "v", "z"), ("c", "o"),
+    ("nf", "v", 0), ("ra", "v"), ("sp", "o", 1, "x"), ("nf", "o", 0), ("zf", "o", 1), ("zf", "o", 2),
+    ("rs1", "v"), ("zf", "v", 2), ("zf", "v", 1), ("sp", "o", 1, "y"), ("ra", "o"), ("sp", "v", 2, "y"),
+    ("sp", "o", 2, "x"), ("sp", "o", 2, "y"), ("sp", "v", 1, "y"), ("rs2", "v"), ("rs1", "o"), ("zf", "o", 3),
+    ("zf", "v", 3), ("sp", "v", 2, "x"), ("rs2", "o"), ("agz", "v", 1), ("sp", "v", 1, "x"), ("dg", "o"),
+    ("agz", "v", 3), ("nf", "v", 1), ("agz", "o", 1), ("dz", "o", 1), ("dg", "v"), ("agn", "o", 0),
+    ("agz", "v", 2), ("agz", "o", 2), ("dz", "o", 2), ("nf", "o", 1), ("agz", "o", 3), ("agn", "v", 3),
+    ("agn", "v", 0), ("sp", "v", 3, "y"), ("dz", "v", 2), ("agn", "v", 1), ("nf", "v", 2), ("nf", "o", 2),
+    ("agn", "o", 2), ("dz", "v", 1), ("dz", "o", 3), ("agn", "v", 2), ("sp", "o", 3, "x"),
+    ("sp", "v", 3, "x"), ("agn", "o", 3), ("dz", "v", 3), ("dirs", "v"), ("up", "v", 1, "c"), ("agn", "o", 1),
+    ("up", "v", 1, "d"), ("nf", "o", 3), ("a", "o", "y"), ("dirs", "o"), ("sp", "o", 3, "y"),
+    ("up", "o", 0, "d"), ("up", "o", 2, "c"), ("up", "o", 1, "c"), ("a", "v", "x"), ("up", "v", 2, "c"),
+    ("up", "v", 0, "d"), ("up", "o", 1, "d"), ("up", "v", 3, "c"), ("up", "o", 2, "d"), ("nf", "v", 3),
+    ("up", "o", 3, "d"), ("up", "v", 2, "d"), ("up", "o", 0, "c"), ("up", "v", 0, "c"), ("up", "o", 3, "c"),
+    ("up", "v", 3, "d"),
 )
 
 
@@ -95,9 +96,9 @@
     v_out, o_out, v_master, o_master, vm_new, vs_new, om_new, os_new,
     vw_in, ow_in, inp, vfac, ocot, ofac, vcot, first, second, vm, vs, om, os_, lam, gain,
     gv, go, heads, proj_v, proj_o,
-    part_v, part_o, got_v, got_o, sum_v, sum_o, col_v, col_o,
+    part_v, part_o, got_v, got_o, mid_v, mid_o, half_v, half_o, sum_v, sum_o, col_v, col_o, keep_v, keep_o,
     dfull_v, dfull_o, turned,
-    wsend, wrecv, drecv, psend, precv, rsend, rrecv, csend, crecv, asend, arecv, insem, rising, falling, corner,
+    wsend, wrecv, drecv, psend, precv, rsend, rrecv, csend, crecv, asend, arecv, insem, rising, falling,
 ):
     me = lax.axis_index("fs")
     tp = lax.axis_index("tp")
@@ -109,7 +110,7 @@
     y = lax.rem(lax.div(me, NX), NY)
     z = lax.div(me, NC)
     ox, oy = 1 - x, 1 - y
-    cut = {"v": width * 7 // 8 // 16 * 16, "o": cols * 7 // 8 // 16 * 16}
+    cut = {"v": width * 7 // 8 // 16 * 16, "o": cols * 13 // 16 // 16 * 16}
     size = {"v": width, "o": cols}
     index = {"v": 0, "o": 1}
     store = {"v": gv, "o": go}
@@ -181,7 +182,6 @@
         when(has_down, lambda: pl.semaphore_wait(rising.at[k], 1))
         when(has_up, lambda: pl.semaphore_wait(falling.at[k], 1))
 
-    pl.semaphore_signal(corner, inc=1, device_id={"fs": to_x})
     steps = max(nz - 2, 0)
     if steps:
         tell(0)
@@ -265,11 +265,11 @@
         low = (total - high.astype(F32)).astype(BF16)
         product = (contract(high, right[...]) + contract(low, right[...])) * scale
         for b in range(nfs):
-            part[b % NC, b // NC] = squared(product[b * rows:(b + 1) * rows])
-        for k in (1, 2, 3):
-            cx = ox if k & 1 else x
-            cy = oy if k & 2 else y
-            send(rsend, kind, part.at[cy * NX + cx], got.at[k], rrecv.at[index[kind], k], at(z, cy, cx))
+            cy, cx = b // NX % NY, b % NX
+            lead, follow = (cx, cy) if kind == "v" else (cy, cx)
+            part[lead, follow, b // NC] = squared(product[b * rows:(b + 1) * rows])
+        other, target = (ox, to_x) if kind == "v" else (oy, to_y)
+        send(rsend, kind, part.at[other], got, rrecv.at[index[kind], 0], target)
 
     def fetch(*names):
         for name in names:
@@ -283,50 +283,69 @@
             mean = jnp.mean(diff * diff, axis=-1, keepdims=True)
             heads[:, span] = (diff * lax.rsqrt(mean + 1e-06) * gain[...]).astype(BF16)
 
-    def compute(kind):
+    def project_once(kind):
+        if kind in pcopies:
+            return
         if kind == "v":
             fetch("inp", "vfac")
             project("v", inp, vfac, proj_v)
+        else:
             fetch("ocot", "ofac")
             project("o", ocot, ofac, proj_o)
+
+    def compute(kind):
+        opening = not pcopies
+        project_once(kind)
+        project_once("o" if kind == "v" else "v")
+        if kind == "v":
             fetch("vcot")
-            pl.semaphore_wait(corner, 1)
+        else:
+            fetch("first", "second", "lam", "gain", "vm", "vs", "om", "os")
+            normalize()
+        if opening:
             for k in range(1, steps):
                 hear(k - 1)
                 tell(k)
+        if kind == "v":
             reduce_low("v", proj_v, vcot, part_v, got_v)
         else:
-            fetch("first", "second", "lam", "gain", "vm", "vs", "om", "os")
-            normalize()
             reduce_low("o", proj_o, heads, part_o, got_o)
 
-    parts = {"v": (part_v, got_v, sum_v, col_v), "o": (part_o, got_o, sum_o, col_o)}
+    parts = {
+        "v": (part_v, got_v, mid_v, half_v, sum_v, col_v, keep_v),
+        "o": (part_o, got_o, mid_o, half_o, sum_o, col_o, keep_o),
+    }
     moments = {"v": (vm, vs, vm_new, vs_new), "o": (om, os_, om_new, os_new)}
     dfull = {"v": dfull_v, "o": dfull_o}
 
     heard = []
 
+    def ra(kind):
+        part, got, mid, half, total, col, keep = parts[kind]
+        landed(got, rrecv.at[index[kind], 0])
+        lead, own, other, target = (x, y, oy, to_y) if kind == "v" else (y, x, ox, to_x)
+        keep[...] = rooted(part[lead, own]) + rooted(got[own])
+        mid[...] = squared(rooted(part[lead, other]) + rooted(got[other]))
+        send(rsend, kind, mid, half, rrecv.at[index[kind], 1], target)
+
     def rs1(kind):
-        part, got, total, col = parts[kind]
+        part, got, mid, half, total, col, keep = parts[kind]
         if steps and not heard:
             hear(steps - 1)
             heard.append(True)
-        for k in (1, 2, 3):
-            landed(got.at[k], rrecv.at[index[kind], k])
-        acc = rooted(part[y * NX + x])
-        for k in (1, 2, 3):
-            acc = acc + rooted(got[k])
-        total[...] = squared(acc)
+        landed(half, rrecv.at[index[kind], 1])
+        keep[...] = keep[...] + rooted(half[...])
+        total[...] = squared(keep[...])
         for d in range(1, nz):
             peer = lax.rem(z + d, nz)
             send(csend, kind, total.at[peer], col.at[d], crecv.at[index[kind], d], at(peer, y, x))
 
     def rs2(kind):
-        part, got, total, col = parts[kind]
+        part, got, mid, half, total, col, keep = parts[kind]
         m_ref, s_ref, m_out, s_out = moments[kind]
         for d in range(1, nz):
             landed(col.at[d], crecv.at[index[kind], d])
-        g = rooted(total[z])
+        g = keep[z]
         for d in range(1, nz):
             g = g + rooted(col[d])
         m = 0.8 * m_ref[...] + 0.2 * g
@@ -474,7 +493,7 @@
 
     ops = {
         "a": own_send, "c": compute, "zf": zf, "sp": sp, "nf": nf, "dg": dg, "dz": dz,
-        "rs1": rs1, "rs2": rs2, "agz": agz, "agn": agn, "dirs": dirs, "up": update,
+        "ra": ra, "rs1": rs1, "rs2": rs2, "agz": agz, "agn": agn, "dirs": dirs, "up": update,
     }
     for name, *args in schedule(nz):
         ops[name](*args)
@@ -529,8 +548,10 @@
         ((nfs, cols, width), BF16),
         ((tokens, cols), BF16),
         *[((ntp, tokens, rank), F32)] * 2,
-        *[((NC, nz, rows, cols), BF16)] * 4,
-        *[((nz, rows, cols), BF16)] * 4,
+        *[((2, 2, nz, rows, cols), BF16)] * 2,
+        *[((2, nz, rows, cols), BF16)] * 2,
+        *[((nz, rows, cols), BF16)] * 8,
+        *[((nz, rows, cols), F32)] * 2,
         *[((nfs, rows, cols), BF16)] * 2,
         ((cols, rank), BF16),
     ]
@@ -548,7 +569,7 @@
             dma((2, NC)), dma((2, NC)),
             dma((2, nz)), dma((2, nz)),
             dma((2, 5 * nz)), dma((2, nfs)), dma((len(operands),)),
-            regular((max(nz - 2, 1),)), regular((max(nz - 2, 1),)), regular,
+            regular((max(nz - 2, 1),)), regular((max(nz - 2, 1),)),
         ],
         compiler_params=pltpu.CompilerParams(collective_id=0, has_side_effects=True, vmem_limit_bytes=VMEM_LIMIT),
     )(

time: 88.4 us -> 85.6 us (0.968)
  Pallas kernels: 87.6 us -> 84.9 us
    pallas_call x1, Pallas kernels: 83.9 us -> 81.1 us  [local(): pl.pallas_call(functools.partial(exchange, nfs, ntp, scale), out_shape=tu...]
where the time goes in v3:
time: 85.6 us; the launch traced here: 85.5 us
  Pallas kernels  84.9 us (99%)
    pallas_call x1, Pallas kernels, local(): pl.pallas_call(functools.partial(exchange, nfs, ntp, scale), out_shape=tu...  81.1 us
    pallas_call x1, Pallas kernels, local(): pl.pallas_call(functools.partial(publish, len(outs)), out_shape=out_shape...  3.72 us

profile of v3, /device:TPU:0, one launch (start us, length us, event | category | flops | bytes accessed | tf_op | source)
XLA Modules:
  0.0 85.5 jit_solution(16677017830805299910)
XLA Ops:
  0.6 81.1 %shard_map.206 = (bf16[2048,1024]{1,0:T(8,128)(2,1)S(1)}, bf16[1024,2048]{1,0:T(8,128)(2,1)S(1)}, f32[128,1024]{1,0:T(8,128)S(1)}, f32[1024,128]{1,0:T(8,128)S(1...) custom-call(f32[128,1024]{1,0:T(8,128)} %vw_hbm.1, ...), custom_call_target="tpu_custom_call" | custom-call | tf_op jit(solution)/shard_map/pallas_call | solution.py:559
  81.8 3.7 %shard_map.207 = (bf16[2048,1024]{1,0:T(8,128)(2,1)}, bf16[1024,2048]{1,0:T(8,128)(2,1)}, f32[128,1024]{1,0:T(8,128)}, f32[1024,128]{1,0:T(8,128)}, f32[16,1024]...) custom-call(bf16[2048,1024]{1,0:T(8,128)(2,1)S(1)} %get-tuple-element.24.refs_0_, ...), custom_call_target="tpu_custom_call" | custom-call | tf_op jit(solution)/shard_map/pallas_call | solution.py:578

commit v4 on v3

--- a/solution.py
+++ b/solution.py
@@ -67,20 +67,20 @@
 
 
 STEPS = (
-    ("a", "v", "y"), ("a", "o", "z"), ("a", "o", "x"), ("c", "v"), ("a", "v", "z"), ("c", "o"),
-    ("nf", "v", 0), ("ra", "v"), ("sp", "o", 1, "x"), ("nf", "o", 0), ("zf", "o", 1), ("zf", "o", 2),
-    ("rs1", "v"), ("zf", "v", 2), ("zf", "v", 1), ("sp", "o", 1, "y"), ("ra", "o"), ("sp", "v", 2, "y"),
-    ("sp", "o", 2, "x"), ("sp", "o", 2, "y"), ("sp", "v", 1, "y"), ("rs2", "v"), ("rs1", "o"), ("zf", "o", 3),
-    ("zf", "v", 3), ("sp", "v", 2, "x"), ("rs2", "o"), ("agz", "v", 1), ("sp", "v", 1, "x"), ("dg", "o"),
-    ("agz", "v", 3), ("nf", "v", 1), ("agz", "o", 1), ("dz", "o", 1), ("dg", "v"), ("agn", "o", 0),
-    ("agz", "v", 2), ("agz", "o", 2), ("dz", "o", 2), ("nf", "o", 1), ("agz", "o", 3), ("agn", "v", 3),
-    ("agn", "v", 0), ("sp", "v", 3, "y"), ("dz", "v", 2), ("agn", "v", 1), ("nf", "v", 2), ("nf", "o", 2),
-    ("agn", "o", 2), ("dz", "v", 1), ("dz", "o", 3), ("agn", "v", 2), ("sp", "o", 3, "x"),
-    ("sp", "v", 3, "x"), ("agn", "o", 3), ("dz", "v", 3), ("dirs", "v"), ("up", "v", 1, "c"), ("agn", "o", 1),
-    ("up", "v", 1, "d"), ("nf", "o", 3), ("a", "o", "y"), ("dirs", "o"), ("sp", "o", 3, "y"),
-    ("up", "o", 0, "d"), ("up", "o", 2, "c"), ("up", "o", 1, "c"), ("a", "v", "x"), ("up", "v", 2, "c"),
-    ("up", "v", 0, "d"), ("up", "o", 1, "d"), ("up", "v", 3, "c"), ("up", "o", 2, "d"), ("nf", "v", 3),
-    ("up", "o", 3, "d"), ("up", "v", 2, "d"), ("up", "o", 0, "c"), ("up", "v", 0, "c"), ("up", "o", 3, "c"),
+    ("a", "o", "x"), ("a", "v", "y"), ("a", "o", "z"), ("a", "v", "z"), ("c", "o"), ("zf", "o", 1),
+    ("nf", "o", 0), ("zf", "o", 2), ("sp", "o", 1, "x"), ("ra", "o"), ("zf", "v", 2), ("zf", "v", 1),
+    ("c", "v"), ("sp", "v", 1, "y"), ("sp", "o", 2, "x"), ("ra", "v"), ("nf", "v", 0), ("sp", "v", 2, "y"),
+    ("rs1", "o"), ("sp", "v", 2, "x"), ("sp", "o", 2, "y"), ("zf", "v", 3), ("rs1", "v"), ("rs2", "o"),
+    ("nf", "v", 2), ("zf", "o", 3), ("agz", "o", 2), ("rs2", "v"), ("sp", "o", 1, "y"), ("agn", "o", 2),
+    ("dg", "v"), ("agz", "o", 1), ("agz", "o", 3), ("agn", "v", 0), ("dg", "o"), ("a", "v", "x"),
+    ("agz", "v", 1), ("nf", "o", 1), ("agn", "o", 3), ("agz", "v", 3), ("agz", "v", 2), ("dz", "o", 2),
+    ("agn", "v", 2), ("agn", "v", 3), ("sp", "o", 3, "y"), ("agn", "v", 1), ("dz", "v", 2),
+    ("sp", "o", 3, "x"), ("dz", "o", 1), ("dirs", "v"), ("dz", "v", 1), ("agn", "o", 0), ("sp", "v", 3, "x"),
+    ("agn", "o", 1), ("sp", "v", 3, "y"), ("a", "o", "y"), ("dz", "o", 3), ("sp", "v", 1, "x"),
+    ("nf", "v", 1), ("dirs", "o"), ("dz", "v", 3), ("up", "v", 0, "c"), ("nf", "o", 2), ("up", "v", 2, "c"),
+    ("up", "v", 0, "d"), ("up", "o", 2, "c"), ("up", "o", 3, "c"), ("up", "o", 1, "d"), ("nf", "o", 3),
+    ("up", "o", 1, "c"), ("up", "v", 2, "d"), ("nf", "v", 3), ("up", "o", 0, "d"), ("up", "v", 3, "c"),
+    ("up", "o", 0, "c"), ("up", "v", 1, "c"), ("up", "v", 1, "d"), ("up", "o", 2, "d"), ("up", "o", 3, "d"),
     ("up", "v", 3, "d"),
 )
 
@@ -213,7 +213,7 @@
         if part is None:
             return ref, wrecv.at[index[kind], b]
         if part == 0:
-            return store[kind].at[b, pl.ds(0, cut[kind])], drecv.at[index[kind], b]
+            return store[kind].at[b, pl.ds(0, cut[kind])], drecv.at[index[kind], lax.div(b, NC)]
         rest = size[kind] - cut[kind]
         return store[kind].at[b, pl.ds(cut[kind], rest)], wrecv.at[index[kind], b]
 
@@ -246,7 +246,7 @@
         for k in range(1, ntp):
             copy = pltpu.make_async_remote_copy(
                 src_ref=proj.at[0], dst_ref=proj.at[k],
-                send_sem=psend.at[index[kind], k], recv_sem=precv.at[index[kind], k],
+                send_sem=psend.at[index[kind], k - 1], recv_sem=precv.at[index[kind], k - 1],
                 device_id={"tp": lax.rem(tp + k, ntp)},
             )
             copy.start()
@@ -338,13 +338,13 @@
         total[...] = squared(keep[...])
         for d in range(1, nz):
             peer = lax.rem(z + d, nz)
-            send(csend, kind, total.at[peer], col.at[d], crecv.at[index[kind], d], at(peer, y, x))
+            send(csend, kind, total.at[peer], col.at[d], crecv.at[index[kind], d - 1], at(peer, y, x))
 
     def rs2(kind):
         part, got, mid, half, total, col, keep = parts[kind]
         m_ref, s_ref, m_out, s_out = moments[kind]
         for d in range(1, nz):
-            landed(col.at[d], crecv.at[index[kind], d])
+            landed(col.at[d], crecv.at[index[kind], d - 1])
         g = keep[z]
         for d in range(1, nz):
             g = g + rooted(col[d])
@@ -555,7 +555,6 @@
         *[((nfs, rows, cols), BF16)] * 2,
         ((cols, rank), BF16),
     ]
-    sends = 4 + 9 * nz
     outs = pl.pallas_call(
         functools.partial(exchange, nfs, ntp, scale),
         out_shape=tuple(pltpu.VMEM(out.shape, out.dtype) for out in out_shape),
@@ -564,11 +563,11 @@
         scratch_shapes=[
             *[space(operand.shape, operand.dtype) for space, operand in zip(spaces, operands)],
             *[pltpu.VMEM(shape, dtype) for shape, dtype in shapes],
-            dma((2, sends)), dma((2, nfs)), dma((2, nfs)),
-            dma((2, ntp)), dma((2, ntp)),
-            dma((2, NC)), dma((2, NC)),
-            dma((2, nz)), dma((2, nz)),
-            dma((2, 5 * nz)), dma((2, nfs)), dma((len(operands),)),
+            dma((2, 5 * nz + 2)), dma((2, nfs)), dma((2, nz)),
+            dma((2, max(ntp - 1, 1))), dma((2, max(ntp - 1, 1))),
+            dma((2, 2)), dma((2, 2)),
+            dma((2, max(nz - 1, 1))), dma((2, max(nz - 1, 1))),
+            dma((2, 4 * nz - 1)), dma((2, nfs)), dma((len(operands),)),
             regular((max(nz - 2, 1),)), regular((max(nz - 2, 1),)),
         ],
         compiler_params=pltpu.CompilerParams(collective_id=0, has_side_effects=True, vmem_limit_bytes=VMEM_LIMIT),

time: 85.6 us -> 84.6 us (0.988)
  Pallas kernels: 84.9 us -> 83.8 us
    pallas_call x1, Pallas kernels: 81.1 us -> 80.1 us  [local(): pl.pallas_call(functools.partial(exchange, nfs, ntp, scale), out_shape=tu...]
where the time goes in v4:
time: 84.6 us; the launch traced here: 84.5 us
  Pallas kernels  83.8 us (99%)
    pallas_call x1, Pallas kernels, local(): pl.pallas_call(functools.partial(exchange, nfs, ntp, scale), out_shape=tu...  80.1 us
    pallas_call x1, Pallas kernels, local(): pl.pallas_call(functools.partial(publish, len(outs)), out_shape=out_shape...  3.72 us

profile of v4, /device:TPU:0, one launch (start us, length us, event | category | flops | bytes accessed | tf_op | source)
XLA Modules:
  0.0 84.5 jit_solution(17936089858238578118)
XLA Ops:
  0.6 80.1 %shard_map.206 = (bf16[2048,1024]{1,0:T(8,128)(2,1)S(1)}, bf16[1024,2048]{1,0:T(8,128)(2,1)S(1)}, f32[128,1024]{1,0:T(8,128)S(1)}, f32[1024,128]{1,0:T(8,128)S(1...) custom-call(f32[128,1024]{1,0:T(8,128)} %vw_hbm.1, ...), custom_call_target="tpu_custom_call" | custom-call | tf_op jit(solution)/shard_map/pallas_call | solution.py:558
  80.8 3.7 %shard_map.207 = (bf16[2048,1024]{1,0:T(8,128)(2,1)}, bf16[1024,2048]{1,0:T(8,128)(2,1)}, f32[128,1024]{1,0:T(8,128)}, f32[1024,128]{1,0:T(8,128)}, f32[16,1024]...) custom-call(bf16[2048,1024]{1,0:T(8,128)(2,1)S(1)} %get-tuple-element.24.refs_0_, ...), custom_call_target="tpu_custom_call" | custom-call | tf_op jit(solution)/shard_map/pallas_call | solution.py:577
